TPU v7x, 32 devices: a whole 2x2x4 slice. The times are simulated.
32 devices in a mesh: fs: 8 (over z, y), tp: 4 (over x, core).
Axes of the slice: x: 2, y: 2, z: 4, core: 2. Of those that a mesh axis runs over, the one named last changes fastest.
Arguments:
- tokens: bfloat16 [8192, 2048], P('fs'), may hold values from -6 to 6
- norm_gain: float32 [2048], replicated, may hold values from 0.1 to 1.9
- gate_weight: bfloat16 [2048, 4096], P('fs', 'tp'), may hold values from -0.125 to 0.125
- up_weight: bfloat16 [2048, 4096], P('fs', 'tp'), may hold values from -0.125 to 0.125
- down_weight: bfloat16 [4096, 2048], P('tp', 'fs'), may hold values from -2 to 2
- out_gain: float32 [2048], P('tp'), may hold values from 0.1 to 1.9
Outputs:
- result: bfloat16 [8192, 2048], P('fs', 'tp')
All inputs are finite; a program needn't handle non-finite values.
Results may differ from a plain program's by a relative error of at most 0.014.
Values may be sent and summed in bfloat16 or wider, within the bound.
No kernel may reach another device: no remote copies, remote signals or barrier semaphores. Data moves between devices by JAX's collectives and lax.ppermute only.
A program may use at most 64 MiB of HBM per device.

v0:
```python
import jax
import jax.numpy as jnp
from jax import lax
from jax.sharding import PartitionSpec as P

EPSILON = 1e-06


def body(tokens, norm_gain, gate_weight, up_weight, down_weight, out_gain):
    values = tokens.astype(jnp.float32)
    normed = (
        values * lax.rsqrt(jnp.mean(values * values, axis=1, keepdims=True) + EPSILON) * norm_gain
    ).astype(jnp.bfloat16)
    gate_all, up_all = (
        lax.all_gather(gate_weight, "fs", axis=0, tiled=True),
        lax.all_gather(up_weight, "fs", axis=0, tiled=True),
    )
    gate_proj = jnp.dot(normed, gate_all, preferred_element_type=jnp.float32)
    up_proj = jnp.dot(normed, up_all, preferred_element_type=jnp.float32)
    hidden = (jax.nn.silu(gate_proj) * up_proj).astype(jnp.bfloat16)
    partial_value = jnp.dot(
        hidden,
        lax.all_gather(down_weight, "fs", axis=1, tiled=True),
        preferred_element_type=jnp.float32,
    )
    own_width = out_gain.shape[0]
    own_columns = lax.psum_scatter(
        partial_value.astype(jnp.bfloat16), "tp", scatter_dimension=1, tiled=True
    ).astype(jnp.float32)
    squares = lax.psum(jnp.sum(own_columns * own_columns, axis=1), "tp")
    mean_square = squares / (own_width * lax.axis_size("tp"))
    scaled = own_columns * lax.rsqrt(mean_square + EPSILON)[:, None] * out_gain[None, :]
    return scaled.astype(jnp.bfloat16)


def solution(mesh):
    return jax.shard_map(
        body,
        mesh=mesh,
        in_specs=(P("fs", None), P(), P("fs", "tp"), P("fs", "tp"), P("tp", "fs"), P("tp")),
        out_specs=P("fs", "tp"),
        check_vma=False,
    )
```

profile of v0, /device:TPU:0, one launch (start us, length us, event | category | flops | bytes accessed | tf_op | source)
XLA Modules:
  0.0 308.2 jit_solution(11775894596299125198)
XLA Ops:
  6.5 0.0 copy-start.1
  6.5 0.0 all-gather.4.cloned.1.call-start
  6.5 0.7 all-gather.4.cloned.1.call-update
  7.3 0.0 all-gather.6.cloned.1.call-start
  7.3 0.7 all-gather.6.cloned.1.call-update
  8.0 0.0 all-gather.8.cloned.1.call-start
  8.1 0.7 all-gather.8.cloned.1.call-update
  8.7 0.0 reduce-scatter.2.cloned.1.call-start
  8.8 3.1 fusion
  11.9 73.1 %all-gather.4.cloned.1.call-done = bf16[2048,1024]{1,0:T(8,128)(2,1)} async-done(((bf16[256,1024]{1,0:T(8,128)(2,1)}), bf16[2048,1024]{1,0:T(8,128)(2,1)}) %all-gather.4.cloned.1.call-update) | async-done | bytes 4194320 | tf_op jit(solution)/shard_map/all_gather | solution.py:15
  85.0 0.0 copy-done.1
  85.0 10.0 %fusion.7 = f32[1024,1024]{1,0:T(8,128)} fusion(bf16[2048,1024]{1,0:T(8,128)(2,1)} %all-gather.4.cloned.1.call-done, bf16[1024,2048]{1,0:T(8,128)(2,1)} %param.6, f32[2048]{0:T(1024)S(1)} %copy-done.1, f32[1024]{0:T(1024)S(1)} %add_rsqrt_fusion.1), kind=kOutput, calls=%fused_computation.12 | convolution fusion | flops 4303355904 | bytes 12595200 | tf_op jit(solution)/shard_map/dot_general | solution.py:18
  95.0 63.5 %all-gather.6.cloned.1.call-done = bf16[2048,1024]{1,0:T(8,128)(2,1)} async-done(((bf16[256,1024]{1,0:T(8,128)(2,1)}), bf16[2048,1024]{1,0:T(8,128)(2,1)}) %all-gather.6.cloned.1.call-update) | async-done | bytes 4194320 | tf_op jit(solution)/shard_map/all_gather | solution.py:16
  158.5 75.3 %all-gather.8.cloned.1.call-done = bf16[1024,2048]{1,0:T(8,128)(2,1)} async-done(((bf16[1024,256]{1,0:T(8,128)(2,1)}), bf16[1024,2048]{1,0:T(8,128)(2,1)}) %all-gather.8.cloned.1.call-update) | async-done | bytes 4194320 | tf_op jit(solution)/shard_map/all_gather | solution.py:23
  233.7 15.3 %convolution_convert_fusion = bf16[1024,2048]{1,0:T(8,128)(2,1)} fusion(bf16[1024,2048]{1,0:T(8,128)(2,1)} %all-gather.8.cloned.1.call-done, f32[1024,1024]{1,0:T(8,128)} %fusion.7, bf16[2048,1024]{1,0:T(8,128)(2,1)} %all-gather.6.cloned.1.call-done, bf16[1024,2048]{1,0:T(8,128)(2,1)} %param.6, f32[2048]{0:T(1024)S(1)} %copy-done.1, ...), kind=kOutput, calls=%fused_computation.6 | convolution fusion | flops 8606711808 | bytes 20983808 | tf_op jit(solution)/shard_map/dot_general | solution.py:21
  249.1 0.0 copy-start
  249.1 0.0 reduce-scatter.2.cloned.1.call-update
  249.1 42.7 %reduce-scatter.2.cloned.1.call-done = bf16[1024,512]{1,0:T(8,128)(2,1)} async-done(((bf16[1024,2048]{1,0:T(8,128)(2,1)}), bf16[1024,512]{1,0:T(8,128)(2,1)}) %reduce-scatter.2.cloned.1.call-update) | async-done | bytes 1048592 | tf_op jit(solution)/shard_map/reduce_scatter | solution.py:27
  291.9 1.5 fusion.3
  293.4 5.8 %psum.7 = f32[1024]{0:T(1024)S(1)} all-reduce(f32[1024]{0:T(1024)S(1)} %fusion.3), channel_id=1, replica_groups=mesh['fs'=8,'tp'=4] {'tp'}, use_global_device_ids=true, to_apply=%region_3.4 | all-reduce | flops 1024 | bytes 8192 | tf_op jit(solution)/shard_map/psum | solution.py:30
  299.1 0.0 copy-done
  299.1 2.5 fusion.5
  (2 shorter events, 0.0 us)
Async XLA Ops:
  6.5 78.5 %copy-start.1 = (f32[2048]{0:T(1024)S(1)}, f32[2048]{0:T(1024)}, u32[]{:S(2)}) copy-start(f32[2048]{0:T(1024)} %param.7) | copy-start | bytes 24580
  6.5 78.5 %all-gather.4.cloned.1.call-start = ((), (), s32[]{:S(2)}) async-start(), calls=%async_computation.1 | async-start | bytes 4718592 | tf_op jit(solution)/shard_map/all_gather | solution.py:15
  7.3 151.2 %all-gather.6.cloned.1.call-start = ((), (), s32[]{:S(2)}) async-start(), calls=%async_computation.2 | async-start | bytes 4718592 | tf_op jit(solution)/shard_map/all_gather | solution.py:16
  8.0 225.7 %all-gather.8.cloned.1.call-start = ((), (), s32[]{:S(2)}) async-start(), calls=%async_computation.3 | async-start | bytes 4718592 | tf_op jit(solution)/shard_map/all_gather | solution.py:23
  8.7 283.1 %reduce-scatter.2.cloned.1.call-start = ((), (), s32[]{:S(2)}) async-start(), calls=%async_computation.4 | async-start | bytes 5242880 | tf_op jit(solution)/shard_map/reduce_scatter | solution.py:27
  249.1 50.0 %copy-start = (f32[512]{0:T(512)S(1)}, f32[512]{0:T(512)}, u32[]{:S(2)}) copy-start(f32[512]{0:T(512)} %param.11) | copy-start | bytes 6148
Sparse Core Ops, SparseCore 0:
  9.5 75.5 all-gather.3
  87.1 71.3 all-gather.5
  160.5 73.1 all-gather.7
  249.2 42.5 reduce-scatter.1
where the time goes:
time: 308 us
  waiting for transfers between devices  257 us (83%)
  matrix products  25.3 us (8%)
  between operations  13.1 us (4%)
  other arithmetic  7.09 us (2%)
  blocking collectives  5.77 us (2%)
    all_gather x1, waiting for transfers between devices, body(): lax.all_gather(down_weight, 'fs', axis=1, tiled=True)  75.3 us
    all_gather x1, waiting for transfers between devices, body(): lax.all_gather(gate_weight, 'fs', axis=0, tiled=True)  73.1 us
    all_gather x1, waiting for transfers between devices, body(): lax.all_gather(up_weight, 'fs', axis=0, tiled=True)  63.5 us
    reduce_scatter x1, waiting for transfers between devices, body(): lax.psum_scatter(partial_value.astype(jnp.bfloat16), 'tp', scatter_dimens...  42.7 us
    dot_general x1, matrix products, body(): jnp.dot(hidden, lax.all_gather(down_weight, 'fs', axis=1, tiled=True), pr...  15.3 us
    dot_general x1, matrix products, body(): gate_proj = jnp.dot(normed, gate_all, preferred_element_type=jnp.float32)  9.96 us
  transfers between devices with their start and end apart: 4, of which 4 were waited for; matrix products, arithmetic and copies ran while one was open for 4% of the time, Pallas kernels for 0%

commit v1 on v0

--- a/solution.py
+++ b/solution.py
@@ -1,3 +1,4 @@
+import functools
 import jax
 import jax.numpy as jnp
 from jax import lax
@@ -6,13 +7,42 @@
 EPSILON = 1e-06
 
 
+def put_links(message, k_dim):
+    message = jnp.moveaxis(message, 0, k_dim)
+    r1 = message.shape
+    return message.reshape(*r1[:k_dim], r1[k_dim] * r1[k_dim + 1], *r1[k_dim + 2 :])
+
+
+def rates_launch(z_in, bus_axis, at_axis):
+    world = lax.psum(1, bus_axis)
+    buffers = list(map(lambda q: (q, (q + 1) % world), range(world)))
+    parts_seen = [(t, ii) for ii, t in buffers]
+    known, block_now = ([], [])
+    ix = 0
+    while ix < world - 1:
+        if ix % 2 == 0:
+            known.append(lax.ppermute(known[-1] if known else z_in, bus_axis, buffers))
+        else:
+            latest = lax.ppermute(block_now[-1] if block_now else z_in, bus_axis, parts_seen)
+            block_now.append(latest)
+        ix += 1
+    x_next = jnp.stack([*known[::-1], z_in, *block_now])
+    oldest = lax.axis_index(bus_axis)
+    y_new = oldest - len(known)
+    x_next = x_next[(jnp.arange(world) - y_new) % world]
+    return put_links(x_next, at_axis)
+
+
+read_columns_for = functools.partial(rates_launch, bus_axis="fs", at_axis=0)
+
+
 def body(tokens, norm_gain, gate_weight, up_weight, down_weight, out_gain):
     values = tokens.astype(jnp.float32)
     normed = (
         values * lax.rsqrt(jnp.mean(values * values, axis=1, keepdims=True) + EPSILON) * norm_gain
     ).astype(jnp.bfloat16)
     gate_all, up_all = (
-        lax.all_gather(gate_weight, "fs", axis=0, tiled=True),
+        read_columns_for(gate_weight),
         lax.all_gather(up_weight, "fs", axis=0, tiled=True),
     )
     gate_proj = jnp.dot(normed, gate_all, preferred_element_type=jnp.float32)

time: 308 us -> 287 us (0.932)
  waiting for transfers between devices: 257 us -> 198 us
  starting transfers between devices: 0.12 us -> 25.3 us
  local copies, waits for them, and re-layouts: 0.01 us -> 11.7 us
    ppermute x0 -> x7, waiting for transfers between devices: none -> 83.9 us  [the longest x4 83.9 us: rates_launch(): known.append(lax.ppermute(known[-1] if known else z_in, bus_axis, buffers))]
    all_gather x1 -> x0, waiting for transfers between devices: 73.1 us -> none  [body(): lax.all_gather(gate_weight, 'fs', axis=0, tiled=True)]
    all_gather x1, waiting for transfers between devices: 63.5 us -> 3.91 us  [body(): lax.all_gather(up_weight, 'fs', axis=0, tiled=True)]
    ppermute x0 -> x7, starting transfers between devices: none -> 25.2 us  [the longest x3 18.7 us: rates_launch(): lax.ppermute(block_now[-1] if block_now else z_in, bus_axis, parts_seen)]
    all_gather x1, waiting for transfers between devices: 75.3 us -> 65.8 us  [body(): lax.all_gather(down_weight, 'fs', axis=1, tiled=True)]
    unnamed x4 -> x13, local copies, waits for them, and re-layouts: 0.01 us -> 5.86 us
    gather x0 -> x1, local copies, waits for them, and re-layouts: none -> 4.98 us  [rates_launch(): x_next = x_next[(jnp.arange(world) - y_new) % world]]
  transfers between devices with their start and end apart: 4 -> 10, of which waited for: 4 -> 7; matrix products, arithmetic and copies ran while one was open for 4% -> 9% of each run, Pallas kernels for 0% -> 0%
where the time goes in v1:
time: 287 us; the launch traced here: 286 us
  waiting for transfers between devices  198 us (69%)
  matrix products  25.6 us (9%)
  starting transfers between devices  25.3 us (9%)
  between operations  13.2 us (5%)
  local copies, waits for them, and re-layouts  11.7 us (4%)
  other arithmetic  7.16 us (2%)
  blocking collectives  5.77 us (2%)
    ppermute x4, waiting for transfers between devices, rates_launch(): known.append(lax.ppermute(known[-1] if known else z_in, bus_axis, buffers))  83.9 us
    all_gather x1, waiting for transfers between devices, body(): lax.all_gather(down_weight, 'fs', axis=1, tiled=True)  65.8 us
    reduce_scatter x1, waiting for transfers between devices, body(): lax.psum_scatter(partial_value.astype(jnp.bfloat16), 'tp', scatter_dimens...  42.7 us
    ppermute x3, starting transfers between devices, rates_launch(): lax.ppermute(block_now[-1] if block_now else z_in, bus_axis, parts_seen)  18.7 us
    dot_general x1, matrix products, body(): jnp.dot(hidden, lax.all_gather(down_weight, 'fs', axis=1, tiled=True), pr...  15.7 us
    dot_general x1, matrix products, body(): up_proj = jnp.dot(normed, up_all, preferred_element_type=jnp.float32)  9.95 us
    ppermute x4, starting transfers between devices, rates_launch(): known.append(lax.ppermute(known[-1] if known else z_in, bus_axis, buffers))  6.49 us
    unnamed x13, local copies, waits for them, and re-layouts  5.86 us
  transfers between devices with their start and end apart: 10, of which 7 were waited for; matrix products, arithmetic and copies ran while one was open for 9% of the time, Pallas kernels for 0%

profile of v1, /device:TPU:0, one launch (start us, length us, event | category | flops | bytes accessed | tf_op | source)
XLA Modules:
  0.0 286.5 jit_solution(4316126266696337796)
XLA Ops:
  8.1 3.0 %collective-permute-start = (bf16[256,1024]{1,0:T(8,128)(2,1)}, bf16[256,1024]{1,0:T(8,128)(2,1)S(1)}, u32[]{:S(2)}, u32[]{:S(2)}) collective-permute-start(bf16[256,1024]{1,0:T(8,128)(2,1)} %param.8), channel_id=1, source_target_pairs={{0,4},{4,8},{8,12},{12,16},{16,20},{20,24},{24,28},{28,0},{1,5},{5... | collective-permute-start | bytes 1572872 | tf_op jit(solution)/shard_map/ppermute | solution.py:24
  11.1 15.7 %collective-permute-done = bf16[256,1024]{1,0:T(8,128)(2,1)S(1)} collective-permute-done((bf16[256,1024]{1,0:T(8,128)(2,1)}, bf16[256,1024]{1,0:T(8,128)(2,1)S(1)}, u32[]{:S(2)}, u32[]{:S(2)}) %collective-permute-start) | collective-permute-done | bytes 524320 | tf_op jit(solution)/shard_map/ppermute | solution.py:24
  26.8 1.0 collective-permute-start.1
  27.8 3.8 %collective-permute-start.4 = (bf16[256,1024]{1,0:T(8,128)(2,1)}, bf16[256,1024]{1,0:T(8,128)(2,1)S(1)}, u32[]{:S(2)}, u32[]{:S(2)}) collective-permute-start(bf16[256,1024]{1,0:T(8,128)(2,1)} %param.8), channel_id=1, source_target_pairs={{4,0},{8,4},{12,8},{16,12},{20,16},{24,20},{28,24},{0,28},{5,1},{9... | collective-permute-start | bytes 1572872 | tf_op jit(solution)/shard_map/ppermute | solution.py:26
  31.5 22.9 %collective-permute-done.1 = bf16[256,1024]{1,0:T(8,128)(2,1)S(1)} collective-permute-done((bf16[256,1024]{1,0:T(8,128)(2,1)S(1)}, bf16[256,1024]{1,0:T(8,128)(2,1)S(1)}, u32[]{:S(2)}, u32[]{:S(2)}) %collective-permute-start.1) | collective-permute-done | bytes 524320 | tf_op jit(solution)/shard_map/ppermute | solution.py:24
  54.5 4.8 %collective-permute-start.5 = (bf16[256,1024]{1,0:T(8,128)(2,1)S(1)}, bf16[256,1024]{1,0:T(8,128)(2,1)S(1)}, u32[]{:S(2)}, u32[]{:S(2)}) collective-permute-start(bf16[256,1024]{1,0:T(8,128)(2,1)S(1)} %collective-permute-done.4), channel_id=1, source_target_pairs={{4,0},{8,4},{12,8},{16,12},{20,16},{24,20},{28,24},{0,28},{5,1},{9... | collective-permute-start | bytes 1572872 | tf_op jit(solution)/shard_map/ppermute | solution.py:26
  59.2 27.4 %collective-permute-done.2 = bf16[256,1024]{1,0:T(8,128)(2,1)S(1)} collective-permute-done((bf16[256,1024]{1,0:T(8,128)(2,1)S(1)}, bf16[256,1024]{1,0:T(8,128)(2,1)S(1)}, u32[]{:S(2)}, u32[]{:S(2)}) %collective-permute-start.2) | collective-permute-done | bytes 524320 | tf_op jit(solution)/shard_map/ppermute | solution.py:24
  86.7 2.5 collective-permute-start.3
  89.1 3.1 %fusion = f32[1024]{0:T(1024)S(1)} fusion(bf16[1024,2048]{1,0:T(8,128)(2,1)} %param.6), kind=kLoop, calls=%fused_computation.3 | loop fusion | flops 6290432 | bytes 4198400 | tf_op jit(solution)/shard_map/reduce_sum | solution.py:42
  92.3 10.2 %collective-permute-start.6 = (bf16[256,1024]{1,0:T(8,128)(2,1)S(1)}, bf16[256,1024]{1,0:T(8,128)(2,1)S(1)}, u32[]{:S(2)}, u32[]{:S(2)}) collective-permute-start(bf16[256,1024]{1,0:T(8,128)(2,1)S(1)} %collective-permute-done.5), channel_id=1, source_target_pairs={{4,0},{8,4},{12,8},{16,12},{20,16},{24,20},{28,24},{0,28},{5,1},{9... | collective-permute-start | bytes 1572872 | tf_op jit(solution)/shard_map/ppermute | solution.py:26
  102.5 17.9 %collective-permute-done.3 = bf16[256,1024]{1,0:T(8,128)(2,1)S(1)} collective-permute-done((bf16[256,1024]{1,0:T(8,128)(2,1)S(1)}, bf16[256,1024]{1,0:T(8,128)(2,1)S(1)}, u32[]{:S(2)}, u32[]{:S(2)}) %collective-permute-start.3) | collective-permute-done | bytes 524320 | tf_op jit(solution)/shard_map/ppermute | solution.py:24
  120.4 0.9 bitcast_dynamic-update-slice_fusion.7
  121.2 0.9 bitcast_dynamic-update-slice_fusion.6
  123.7 0.8 bitcast_dynamic-update-slice_fusion.3
  126.2 0.8 bitcast_dynamic-update-slice_fusion
  127.1 5.0 %gather_fusion = bf16[8,256,1024]{2,1,0:T(8,128)(2,1)} fusion(bf16[8,256,1024]{2,1,0:T(8,128)(2,1)} %bitcast_dynamic-update-slice_fusion, s32[1024]{0:T(1024)S(1)} %pad_clamp_fusion), kind=kCustom, calls=%fused_computation | custom fusion | bytes 8388640 | tf_op jit(solution)/shard_map/gather | solution.py:32
  132.0 3.9 %all-gather.3.cloned.1.call-done = bf16[2048,1024]{1,0:T(8,128)(2,1)} async-done(((bf16[256,1024]{1,0:T(8,128)(2,1)}), bf16[2048,1024]{1,0:T(8,128)(2,1)}) %all-gather.3.cloned.1.call-update) | async-done | bytes 4194320 | tf_op jit(solution)/shard_map/all_gather | solution.py:46
  136.0 9.9 %fusion.7 = f32[1024,1024]{1,0:T(8,128)} fusion(bf16[2048,1024]{1,0:T(8,128)(2,1)} %all-gather.3.cloned.1.call-done, bf16[1024,2048]{1,0:T(8,128)(2,1)} %param.6, f32[2048]{0:T(1024)S(1)} %copy-done.2, f32[1024]{0:T(1024)S(1)} %add_rsqrt_fusion.1), kind=kOutput, calls=%fused_computation.14 | convolution fusion | flops 4303355904 | bytes 12595200 | tf_op jit(solution)/shard_map/dot_general | solution.py:49
  145.9 65.8 %all-gather.5.cloned.1.call-done = bf16[1024,2048]{1,0:T(8,128)(2,1)} async-done(((bf16[1024,256]{1,0:T(8,128)(2,1)}), bf16[1024,2048]{1,0:T(8,128)(2,1)}) %all-gather.5.cloned.1.call-update) | async-done | bytes 4194320 | tf_op jit(solution)/shard_map/all_gather | solution.py:53
  211.7 15.7 %convolution_convert_fusion = bf16[1024,2048]{1,0:T(8,128)(2,1)} fusion(bf16[1024,2048]{1,0:T(8,128)(2,1)} %all-gather.5.cloned.1.call-done, f32[1024,1024]{1,0:T(8,128)} %fusion.7, bf16[2048,1024]{1,0:T(8,128)(2,1)} %bitcast.22, bf16[1024,2048]{1,0:T(8,128)(2,1)} %param.6, f32[2048]{0:T(1024)S(1)} %copy-done.2, f32[1024]{0:T(1024)S(1)} %add_rsqrt_fusion.1), kind=kOutput, calls=%fused_computation.7 | convolution fusion | flops 8606711808 | bytes 20983808 | tf_op jit(solution)/shard_map/dot_general | solution.py:51
  227.4 42.7 %reduce-scatter.2.cloned.1.call-done = bf16[1024,512]{1,0:T(8,128)(2,1)} async-done(((bf16[1024,2048]{1,0:T(8,128)(2,1)}), bf16[1024,512]{1,0:T(8,128)(2,1)}) %reduce-scatter.2.cloned.1.call-update) | async-done | bytes 1048592 | tf_op jit(solution)/shard_map/reduce_scatter | solution.py:57
  270.2 1.5 fusion.3
  271.7 5.8 %psum.7 = f32[1024]{0:T(1024)S(1)} all-reduce(f32[1024]{0:T(1024)S(1)} %fusion.3), channel_id=1, replica_groups=mesh['fs'=8,'tp'=4] {'tp'}, use_global_device_ids=true, to_apply=%region_3.4 | all-reduce | flops 1024 | bytes 8192 | tf_op jit(solution)/shard_map/psum | solution.py:60
  277.5 2.5 fusion.5
  (24 shorter events, 4.9 us)
Async XLA Ops:
  6.5 129.4 %all-gather.3.cloned.1.call-start = ((), (), s32[]{:S(2)}) async-start(), calls=%async_computation.1 | async-start | bytes 4718592 | tf_op jit(solution)/shard_map/all_gather | solution.py:46
  7.3 204.5 %all-gather.5.cloned.1.call-start = ((), (), s32[]{:S(2)}) async-start(), calls=%async_computation.2 | async-start | bytes 4718592 | tf_op jit(solution)/shard_map/all_gather | solution.py:53
  8.0 262.2 %reduce-scatter.2.cloned.1.call-start = ((), (), s32[]{:S(2)}) async-start(), calls=%async_computation.3 | async-start | bytes 5242880 | tf_op jit(solution)/shard_map/reduce_scatter | solution.py:57
  8.1 18.8 %collective-permute-start = (bf16[256,1024]{1,0:T(8,128)(2,1)}, bf16[256,1024]{1,0:T(8,128)(2,1)S(1)}, u32[]{:S(2)}, u32[]{:S(2)}) collective-permute-start(bf16[256,1024]{1,0:T(8,128)(2,1)} %param.8), channel_id=1, source_target_pairs={{0,4},{4,8},{8,12},{12,16},{16,20},{20,24},{24,28},{28,0},{1,5},{5... | collective-permute-start | bytes 1572872 | tf_op jit(solution)/shard_map/ppermute | solution.py:24
  26.8 27.6 %collective-permute-start.1 = (bf16[256,1024]{1,0:T(8,128)(2,1)S(1)}, bf16[256,1024]{1,0:T(8,128)(2,1)S(1)}, u32[]{:S(2)}, u32[]{:S(2)}) collective-permute-start(bf16[256,1024]{1,0:T(8,128)(2,1)S(1)} %collective-permute-done), channel_id=1, source_target_pairs={{0,4},{4,8},{8,12},{12,16},{16,20},{20,24},{24,28},{28,0},{1,5},{5... | collective-permute-start | bytes 1572872 | tf_op jit(solution)/shard_map/ppermute | solution.py:24
  27.8 26.7 %collective-permute-start.4 = (bf16[256,1024]{1,0:T(8,128)(2,1)}, bf16[256,1024]{1,0:T(8,128)(2,1)S(1)}, u32[]{:S(2)}, u32[]{:S(2)}) collective-permute-start(bf16[256,1024]{1,0:T(8,128)(2,1)} %param.8), channel_id=1, source_target_pairs={{4,0},{8,4},{12,8},{16,12},{20,16},{24,20},{28,24},{0,28},{5,1},{9... | collective-permute-start | bytes 1572872 | tf_op jit(solution)/shard_map/ppermute | solution.py:26
  54.4 32.2 %collective-permute-start.2 = (bf16[256,1024]{1,0:T(8,128)(2,1)S(1)}, bf16[256,1024]{1,0:T(8,128)(2,1)S(1)}, u32[]{:S(2)}, u32[]{:S(2)}) collective-permute-start(bf16[256,1024]{1,0:T(8,128)(2,1)S(1)} %collective-permute-done.1), channel_id=1, source_target_pairs={{0,4},{4,8},{8,12},{12,16},{16,20},{20,24},{24,28},{28,0},{1,5},{5... | collective-permute-start | bytes 1572872 | tf_op jit(solution)/shard_map/ppermute | solution.py:24
  54.4 69.3 %copy-start = (bf16[256,1024]{1,0:T(8,128)(2,1)S(1)}, bf16[256,1024]{1,0:T(8,128)(2,1)}, u32[]{:S(2)}) copy-start(bf16[256,1024]{1,0:T(8,128)(2,1)} %param.8) | copy-start | bytes 1572868
  54.5 37.8 %collective-permute-start.5 = (bf16[256,1024]{1,0:T(8,128)(2,1)S(1)}, bf16[256,1024]{1,0:T(8,128)(2,1)S(1)}, u32[]{:S(2)}, u32[]{:S(2)}) collective-permute-start(bf16[256,1024]{1,0:T(8,128)(2,1)S(1)} %collective-permute-done.4), channel_id=1, source_target_pairs={{4,0},{8,4},{12,8},{16,12},{20,16},{24,20},{28,24},{0,28},{5,1},{9... | collective-permute-start | bytes 1572872 | tf_op jit(solution)/shard_map/ppermute | solution.py:26
  86.7 33.7 %collective-permute-start.3 = (bf16[256,1024]{1,0:T(8,128)(2,1)S(1)}, bf16[256,1024]{1,0:T(8,128)(2,1)S(1)}, u32[]{:S(2)}, u32[]{:S(2)}) collective-permute-start(bf16[256,1024]{1,0:T(8,128)(2,1)S(1)} %collective-permute-done.2), channel_id=1, source_target_pairs={{0,4},{4,8},{8,12},{12,16},{16,20},{20,24},{24,28},{28,0},{1,5},{5... | collective-permute-start | bytes 1572872 | tf_op jit(solution)/shard_map/ppermute | solution.py:24
  92.3 34.0 %collective-permute-start.6 = (bf16[256,1024]{1,0:T(8,128)(2,1)S(1)}, bf16[256,1024]{1,0:T(8,128)(2,1)S(1)}, u32[]{:S(2)}, u32[]{:S(2)}) collective-permute-start(bf16[256,1024]{1,0:T(8,128)(2,1)S(1)} %collective-permute-done.5), channel_id=1, source_target_pairs={{4,0},{8,4},{12,8},{16,12},{20,16},{24,20},{28,24},{0,28},{5,1},{9... | collective-permute-start | bytes 1572872 | tf_op jit(solution)/shard_map/ppermute | solution.py:26
  127.1 8.9 %copy-start.2 = (f32[2048]{0:T(1024)S(1)}, f32[2048]{0:T(1024)}, u32[]{:S(2)}) copy-start(f32[2048]{0:T(1024)} %param.7) | copy-start | bytes 24580
  227.4 50.0 %copy-start.1 = (f32[512]{0:T(512)S(1)}, f32[512]{0:T(512)}, u32[]{:S(2)}) copy-start(f32[512]{0:T(512)} %param.11) | copy-start | bytes 6148
Sparse Core Ops, SparseCore 0:
  9.5 126.4 all-gather.2
  138.0 73.6 all-gather.4
  227.6 42.5 reduce-scatter.1
